TPU v7x, 32 devices: a whole 2x2x4 slice. The times are simulated.
32 devices in a mesh: ep: 4 (over y, x), tp: 8 (over z, core).
Axes of the slice: x: 2, y: 2, z: 4, core: 2. Of those that a mesh axis runs over, the one named last changes fastest.
Arguments:
- mixer_input_rows: bfloat16 [4096, 2048], P(('ep', 'tp')), may hold values from -6 to 6
- mixer_norm_gain: float32 [2048], replicated, may hold values from 0.1 to 1.9
- query_weight: bfloat16 [2048, 2048], P(None, 'tp'), may hold values from -0.125 to 0.125
- key_weight: bfloat16 [2048, 2048], P(None, 'tp'), may hold values from -0.125 to 0.125
- value_weight: bfloat16 [2048, 2048], P(None, 'tp'), may hold values from -0.125 to 0.125
- write_strength_projection: bfloat16 [2048, 16], replicated, may hold values from -0.125 to 0.125
- decay_projection: bfloat16 [2048, 16], replicated, may hold values from -0.125 to 0.125
- head_decay_speed: float32 [16], P('tp'), may hold values from 0 to 1
- largest_write_strength: float32 [16], P('tp'), may hold values from 0 to 1
- extra_log_decay: float32 [4096, 16], P('ep', 'tp'), may hold values from -1 to 0
- head_norm_gain: float32 [128], replicated, may hold values from 0.1 to 1.9
- mixer_output_weight: bfloat16 [2048, 2048], P('tp'), may hold values from -0.125 to 0.125
- expert_input_rows: bfloat16 [256, 2048], P(('ep', 'tp')), may hold values from -6 to 6
- expert_norm_gain: float32 [2048], replicated, may hold values from 0.1 to 1.9
- routes: int32 [256, 2], P(('ep', 'tp')), may hold values from 0 to 3, all different within a row; in each aligned block of 8 rows (0 to 7, 8 to 15, ...) at most 6 rows name the same one
- expert_route_weight: float32 [256, 2], P(('ep', 'tp')), may hold values from 0.2 to 1
- gate_weight: bfloat16 [4, 2048, 7168], P('ep', None, 'tp'), may hold values from -0.125 to 0.125
- up_weight: bfloat16 [4, 2048, 7168], P('ep', None, 'tp'), may hold values from -0.125 to 0.125
- down_weight: bfloat16 [4, 7168, 2048], P('ep', 'tp'), may hold values from -0.0625 to 0.0625
Outputs:
- mix_out: bfloat16 [4096, 2048], P(('ep', 'tp'))
- exp_out: bfloat16 [256, 2048], P(('ep', 'tp'))
Inputs may be any that keep to these rules, and one draw needn't show every extreme that they name: `routes`: within the rows of one device (aligned blocks of 8 rows) no expert is named more than 6 times, some device names some expert exactly 6 times, and the 2 experts of a row differ.
All inputs are finite; a program needn't handle non-finite values.
Results may differ from a plain program's by a relative error of at most 0.019.
Values may be sent and summed in bfloat16 or wider, within the bound.
A program may use at most 128 MiB of HBM per device.

v0:
```python
import functools

import jax
import jax.numpy as jnp
from jax import lax
from jax.experimental import pallas as pl
from jax.experimental.pallas import tpu as pltpu
from jax.sharding import PartitionSpec as P

HEAD = 128
BLOCK = 128
CORES = 2

norm_eps = 1e-06
highest = lax.Precision.HIGHEST
f32 = jnp.float32
bf16 = jnp.bfloat16


def narrow(x):
    return x.astype(bf16)


def halves(x):
    top = narrow(x)
    return top, narrow(x - top.astype(f32))


def mm(a, b):
    return jnp.dot(a, b, preferred_element_type=f32)


def mm_nt(a, b):
    return lax.dot_general(a, b, (((1,), (1,)), ((), ())), preferred_element_type=f32)


def square_full(a, b):
    a_top, a_low = halves(a)
    b_top, b_low = halves(b)
    wide = jnp.concatenate([b_top, b_low], axis=1)
    both = mm(
        jnp.concatenate([a_top, a_low], axis=1), jnp.concatenate([wide, wide], axis=0)
    )
    return both[:, : b.shape[1]] + both[:, b.shape[1] :]


def wide_full(a, b):
    a_top, a_low = halves(a)
    b_top, b_low = halves(b)
    return mm(
        jnp.concatenate([a_top, a_low], axis=1), jnp.concatenate([b_top, b_top], axis=0)
    ) + mm(a_top, b_low)


def silu(x):
    return x / (1.0 + jnp.exp(-x))


def rms_rows(rows, gain):
    wide = rows.astype(f32)
    return wide * lax.rsqrt(jnp.mean(wide * wide, axis=-1, keepdims=True) + norm_eps) * gain


def fused_kernel(
    sizes,
    x_ref,
    xgain_ref,
    w8_ref,
    prm_ref,
    extra_ref,
    hgain_ref,
    tok_ref,
    tgain_ref,
    share_ref,
    wq_hbm,
    wk_hbm,
    wv_hbm,
    wo_hbm,
    wg_hbm,
    wu_hbm,
    wd_hbm,
    mix_ref,
    exp_ref,
    wq_ref,
    wk_ref,
    wv_ref,
    wg_ref,
    wu_ref,
    wd_ref,
    rows_all,
    wo_all,
    tok_all,
    part_all,
    part_in,
    line_all,
    line_in,
    own_all,
    query_all,
    pair_all,
    prefix_all,
    run_ref,
    span_out,
    span_in,
    memory_ref,
    mixed_all,
    mixed_in,
    local_sem,
    r_s,
    r_r,
    rs_s,
    rs_r,
    w_s,
    w_r,
    wx_s,
    wx_r,
    ws_s,
    ws_r,
    t_s,
    t_r,
    te_s,
    te_r,
    ts_s,
    ts_r,
    st_s,
    st_r,
    p_s,
    p_r,
    l_s,
    l_r,
    a_s,
    a_r,
):
    EP, Z, H = sizes
    T = Z * CORES
    e = lax.axis_index("ep")
    t = lax.axis_index("tp")
    z = t // CORES
    c = t % CORES
    width = H * HEAD
    model = x_ref.shape[1]
    piece = model // EP
    half = model // 2
    hp = w8_ref.shape[0] // 2

    def remote(src, dst, s, r, **where):
        return pltpu.make_async_remote_copy(
            src_ref=src,
            dst_ref=dst,
            send_sem=s,
            recv_sem=r,
            device_id=where,
            device_id_type=pl.DeviceIdType.MESH,
        )

    def start(copy):
        copy.start()

    def done_send(copy):
        copy.wait_send()

    def done_recv(copy):
        copy.wait_recv()

    def row_copy(zz, step):
        slot = rows_all.at[zz, c]
        d = 0 if step > 0 else 1
        return remote(slot, slot, r_s.at[d, zz], r_r.at[zz], tp=t + step * CORES)

    def row_sibling(zz, core):
        slot = rows_all.at[zz, core]
        return remote(slot, slot, rs_s.at[zz], rs_r.at[zz], tp=z * CORES + 1 - c)

    def wo_slot(zz, core, ee):
        return wo_all.at[zz, core, :, pl.ds(pl.multiple_of(ee * piece, piece), piece)]

    def wo_copy(zz, step):
        slot = wo_slot(zz, c, e)
        d = 0 if step > 0 else 1
        return remote(slot, slot, w_s.at[d, zz], w_r.at[zz], tp=t + step * CORES)

    def wo_peer(zz, frm, to):
        slot = wo_slot(zz, c, frm)
        return remote(slot, slot, wx_s.at[zz, to], wx_r.at[zz, frm], ep=to)

    def wo_sibling(zz, core):
        slot = wo_all.at[zz, core]
        return remote(slot, slot, ws_s.at[zz], ws_r.at[zz], tp=z * CORES + 1 - c)

    def tok_copy(frm, to):
        slot = tok_all.at[e, c, frm]
        return remote(slot, slot, t_s.at[to], t_r.at[frm], tp=to * CORES + c)

    def tok_peer(frm, to):
        slot = tok_all.at[frm, c]
        return remote(slot, slot, te_s.at[to], te_r.at[frm], ep=to)

    def tok_sibling(ee, core):
        slot = tok_all.at[ee, core]
        return remote(slot, slot, ts_s.at[ee], ts_r.at[ee], tp=z * CORES + 1 - c)

    def state_copy(frm, to):
        return remote(span_out, span_in.at[frm], st_s.at[to], st_r.at[frm], ep=to)

    def part_copy(frm, to):
        return remote(part_all.at[to], part_in.at[frm], p_s.at[to], p_r.at[frm], ep=to)

    def line_copy(frm, to):
        return remote(
            line_all.at[to % CORES, to // CORES],
            line_in.at[frm],
            l_s.at[to],
            l_r.at[frm],
            tp=to,
        )

    def mixed_slot(frm):
        return mixed_in.at[:, pl.ds(pl.multiple_of(frm * width, HEAD), width)]

    def mixed_copy(frm, to):
        return remote(mixed_all.at[to], mixed_slot(frm), a_s.at[to], a_r.at[frm], tp=to)

    def eps(other, act):
        for ee in range(EP):
            pl.when(other(ee))(functools.partial(act, ee))

    def tps(act):
        for tt in range(T):
            pl.when(t != tt)(functools.partial(act, tt))

    def zs(act):
        for zz in range(Z):
            pl.when(z != zz)(functools.partial(act, zz))

    others = lambda ee: e != ee

    loads = [
        pltpu.make_async_copy(src, dst, local_sem.at[i])
        for i, (src, dst) in enumerate(
            [
                (wq_hbm, wq_ref),
                (wk_hbm, wk_ref),
                (wv_hbm, wv_ref),
                (wo_hbm, wo_all.at[z, c]),
                (wg_hbm.at[0], wg_ref),
                (wu_hbm.at[0], wu_ref),
                (wd_hbm.at[0], wd_ref),
            ]
        )
    ]
    for load in loads:
        load.start()

    barrier = pltpu.get_barrier_semaphore()

    def greet_tp(tt):
        pl.semaphore_signal(barrier, inc=1, device_id={"tp": tt}, device_id_type=pl.DeviceIdType.MESH)

    def greet_ep(ee):
        pl.semaphore_signal(barrier, inc=1, device_id={"ep": ee}, device_id_type=pl.DeviceIdType.MESH)

    tps(greet_tp)
    eps(others, greet_ep)

    rows_all[z, c] = narrow(rms_rows(x_ref[...], xgain_ref[...]))
    tokens = rms_rows(tok_ref[...], tgain_ref[...])
    share = share_ref[...]
    share_top = narrow(share).astype(f32)
    tok_all[e, c, z] = narrow(
        jnp.concatenate(
            [
                jnp.concatenate([tokens[:, :half], share_top], axis=1),
                jnp.concatenate([tokens[:, half:], share - share_top], axis=1),
            ],
            axis=0,
        )
    )
    pl.semaphore_wait(barrier, T - 1 + EP - 1)

    zs(lambda zz: start(tok_copy(z, zz)))

    def row_forward(zz):
        pl.when((zz <= z) & (z + 1 < Z))(lambda: start(row_copy(zz, 1)))
        pl.when((zz >= z) & (z >= 1))(lambda: start(row_copy(zz, -1)))
        start(row_sibling(zz, c))

    def row_arrive(zz):
        done_recv(row_copy(zz, 1))
        row_forward(zz)

    def wo_forward(zz):
        pl.when((zz <= z) & (z + 1 < Z))(lambda: start(wo_copy(zz, 1)))
        pl.when((zz >= z) & (z >= 1))(lambda: start(wo_copy(zz, -1)))

    def wo_arrive(zz):
        done_recv(wo_copy(zz, 1))
        wo_forward(zz)
        eps(others, lambda ee: start(wo_peer(zz, e, ee)))

    def wo_collect(zz):
        eps(others, lambda ee: done_recv(wo_peer(zz, ee, ee)))
        start(wo_sibling(zz, c))

    def both_sides(s, act):
        pl.when(z - s >= 0)(lambda: act(z - s))
        pl.when(z + s < Z)(lambda: act(z + s))

    for load in loads[:4]:
        load.wait()

    row = lax.broadcasted_iota(jnp.int32, (BLOCK, BLOCK), 0)
    col = lax.broadcasted_iota(jnp.int32, (BLOCK, BLOCK), 1)

    def process(zz):
        causal = row >= col
        strict = row > col
        eye = (row == col).astype(f32)
        upper = (row <= col).astype(f32)
        rows = rows_all[zz].reshape(CORES * BLOCK, model)
        q_all = silu(mm(rows, wq_ref[...]))
        k_all = silu(mm(rows, wk_ref[...]))
        v_all = silu(mm(rows, wv_ref[...]))
        small = mm_nt(w8_ref[...], rows)
        at_rows = pl.ds(pl.multiple_of(zz * CORES * BLOCK, CORES * BLOCK), CORES * BLOCK)
        scale = prm_ref[:, :1]
        strength_rows = scale / (1.0 + jnp.exp(-small))
        softplus = jnp.maximum(small, 0.0) + jnp.log1p(jnp.exp(-jnp.abs(small)))
        decay_rows = extra_ref[:, at_rows] - scale * softplus
        chains = []
        for b in range(CORES):
            at = slice(b * BLOCK, (b + 1) * BLOCK)
            across = jnp.dot(
                decay_rows[:, at], upper, preferred_element_type=f32, precision=highest
            )
            cumulative = across.T
            betas = strength_rows[:, at].T
            for h in range(H):
                of = slice(h * HEAD, (h + 1) * HEAD)
                g = hp + h
                cc = cumulative[:, g : g + 1]
                k = k_all[at, of]
                k = k * lax.rsqrt(jnp.sum(k * k, axis=1, keepdims=True) + 1e-06)
                decays = jnp.exp(jnp.where(causal, cc - across[g : g + 1, :], -1e30))
                chains.append(
                    dict(
                        b=b,
                        h=h,
                        q=q_all[at, of],
                        k=k,
                        v=v_all[at, of],
                        beta=betas[:, h : h + 1],
                        c=cc,
                        decays=decays,
                        last=cumulative[BLOCK - 1 : BLOCK, g : g + 1],
                    )
                )
        for m in chains:
            m["kt"] = m["k"].T
        for m in chains:
            inner = square_full(m["k"], m["kt"])
            m["low"] = jnp.where(strict, inner * m["decays"] * m["beta"], 0.0)
            m["scores"] = narrow(mm(narrow(m["q"]), narrow(m["kt"])) * m["decays"])
        pair_mask = strict & (row // 2 == col // 2)
        for m in chains:
            m["inv"] = eye - jnp.where(pair_mask, m["low"], 0.0)
        size = 2
        while size < BLOCK:
            mask = (row // (2 * size) == col // (2 * size)) & (row // size > col // size)
            for m in chains:
                m["tmp"] = square_full(jnp.where(mask, m["low"], 0.0), m["inv"])
            for m in chains:
                m["inv"] = m["inv"] - square_full(m["inv"], m["tmp"])
            size *= 2
        for m in chains:
            grown = jnp.exp(m["c"])
            m["grown"] = grown
            right = jnp.concatenate(
                [m["v"] * m["beta"], m["k"] * (m["beta"] * grown)], axis=1
            )
            m["solved"] = wide_full(m["inv"], right)
        for m in chains:
            keys_dec_t = (m["k"] * jnp.exp(m["last"] - m["c"])).T
            moved = wide_full(keys_dec_t, m["solved"])
            m["shift"] = moved[:, :HEAD]
            m["map"] = eye * jnp.exp(m["last"]) - moved[:, HEAD:]
            read = mm(m["scores"], narrow(m["solved"]))
            m["own"] = read[:, :HEAD]
            m["query"] = m["q"] * m["grown"] - read[:, HEAD:]
        state = [None] * H
        for m in chains:
            b, h = m["b"], m["h"]
            at, of = slice(b * BLOCK, (b + 1) * BLOCK), slice(h * HEAD, (h + 1) * HEAD)
            if state[h] is None:
                own_all[zz, at, of] = m["own"]
                query_all[zz, at, of] = narrow(m["query"])
                state[h] = jnp.concatenate([m["shift"], m["map"]], axis=1)
            else:
                out = mm(narrow(m["query"]), narrow(state[h]))
                own_all[zz, at, of] = out[:, :HEAD] + m["own"]
                query_all[zz, at, of] = narrow(out[:, HEAD:])
                later = wide_full(m["map"], state[h])
                state[h] = jnp.concatenate(
                    [later[:, :HEAD] + m["shift"], later[:, HEAD:]], axis=1
                )
        for h in range(H):
            pair_all[zz, h] = state[h]

    lines = max(1, min(EP, (2 * BLOCK) // (8 * T)))

    def experts():
        for load in loads[4:]:
            load.wait()
        eps(lambda ee: e >= 0, lambda ee: done_recv(tok_sibling(ee, 1 - c)))
        lane = lax.broadcasted_iota(jnp.int32, (lines * T, 16, HEAD), 2)

        def chunk(i, _):
            span = pl.ds(i * lines, lines)
            got = tok_all[span].reshape(lines * T, 16, half + HEAD).astype(f32)
            count = lines * T * 8
            rows = narrow(
                jnp.concatenate(
                    [
                        got[:, :8, :half].reshape(count, half),
                        got[:, 8:, :half].reshape(count, half),
                    ],
                    axis=1,
                )
            )
            weigh = jnp.sum(
                jnp.where(lane == e, got[:, :, half:], 0.0), axis=2, keepdims=True
            )
            weigh = (weigh[:, :8] + weigh[:, 8:]).reshape(count, 1)
            hidden = narrow(silu(mm(rows, wg_ref[...])) * mm(rows, wu_ref[...]))
            partial = (mm(hidden, wd_ref[...]) * weigh).reshape(lines * T, 8, model)
            part_all[span] = narrow(
                jnp.concatenate([partial[:, :, :half], partial[:, :, half:]], axis=1)
            ).reshape(lines, CORES, Z, 16, half)
            return 0

        lax.fori_loop(0, EP // lines, chunk, 0)

    mid = min(2, Z - 1)

    def step(s, _):
        @pl.when(s == 0)
        def _():
            row_forward(z)

        @pl.when(s >= 1)
        def _():
            both_sides(s, row_arrive)

        @pl.when(s == 1)
        def _():
            wo_forward(z)
            start(wo_sibling(z, c))
            zs(lambda zz: done_recv(tok_copy(zz, zz)))
            eps(others, lambda ee: start(tok_peer(e, ee)))

        @pl.when(s >= 2)
        def _():
            both_sides(s - 1, wo_arrive)

        @pl.when(s == mid)
        def _():
            eps(others, lambda ee: done_recv(tok_peer(ee, ee)))
            eps(lambda ee: e >= 0, lambda ee: start(tok_sibling(ee, c)))

        def side(d, _):
            zz = jnp.where(d == 0, z - s, z + s)

            @pl.when((zz >= 0) & (zz < Z) & ((s > 0) | (d == 0)))
            def _():
                done_recv(row_sibling(zz, 1 - c))
                process(zz)

            return 0

        lax.fori_loop(0, 2, side, 0)

        pl.when(s == max(mid, Z - 2))(experts)
        return 0

    lax.fori_loop(0, Z, step, 0)

    for h in range(H):
        run_ref[h] = pair_all[0, h]

    def compose(zz, _):
        for h in range(H):
            now = run_ref[h]
            prefix_all[zz, h] = narrow(now)
            mine = pair_all[zz, h]
            later = wide_full(mine[:, HEAD:], now)
            run_ref[h] = jnp.concatenate(
                [later[:, :HEAD] + mine[:, :HEAD], later[:, HEAD:]], axis=1
            )
        return 0

    lax.fori_loop(1, Z, compose, 0)
    for h in range(H):
        span_out[h] = narrow(run_ref[h])
    eps(lambda ee: e < ee, lambda ee: start(state_copy(e, ee)))
    eps(others, lambda ee: start(part_copy(e, ee)))
    both_sides(Z - 1, wo_arrive)
    for s in range(1, Z - 1):
        both_sides(s, wo_collect)

    def extend(zz, _):
        for h in range(H):
            of = slice(h * HEAD, (h + 1) * HEAD)
            out = mm(query_all[zz, :, of], prefix_all[zz, h])
            own_all[zz, :, of] += out[:, :HEAD]
            query_all[zz, :, of] = narrow(out[:, HEAD:])
        return 0

    lax.fori_loop(1, Z, extend, 0)

    memory_ref[...] = jnp.zeros_like(memory_ref)

    def enter(ee):
        done_recv(state_copy(ee, ee))
        for h in range(H):
            top, low = halves(memory_ref[h])
            theirs = span_in[ee, h]
            span_map = theirs[:, HEAD:]
            memory_ref[h] = (
                theirs[:, :HEAD].astype(f32) + mm(span_map, top) + mm(span_map, low)
            )

    for ee in range(EP - 1):
        pl.when(ee < e)(functools.partial(enter, ee))

    def finish(zz, _):
        for h in range(H):
            of = slice(h * HEAD, (h + 1) * HEAD)
            top, low = halves(memory_ref[h])
            both = mm(query_all[zz, :, of], jnp.concatenate([top, low], axis=1))
            heads = own_all[zz, :, of] + both[:, :HEAD] + both[:, HEAD:]
            scale = lax.rsqrt(jnp.mean(heads * heads, axis=1, keepdims=True) + norm_eps)
            done = narrow(heads * scale * hgain_ref[...])
            for b in range(CORES):
                mixed_all[zz * CORES + b, :, of] = done[b * BLOCK : (b + 1) * BLOCK]
        return 0

    lax.fori_loop(0, Z, finish, 0)
    tps(lambda tt: start(mixed_copy(t, tt)))
    mine = pltpu.make_async_copy(mixed_all.at[t], mixed_slot(t), local_sem.at[7])
    mine.start()

    total = part_all[e].astype(f32)
    part_in[e] = jnp.zeros_like(part_in[e])
    eps(others, lambda ee: done_recv(part_copy(ee, ee)))
    for ee in range(EP):
        total = total + part_in[ee].astype(f32)
    line_all[...] = narrow(total)
    line_in[t] = line_all[c, z]
    tps(lambda tt: start(line_copy(t, tt)))

    both_sides(Z - 1, wo_collect)
    zs(lambda zz: done_recv(wo_sibling(zz, 1 - c)))
    done_recv(wo_sibling(z, 1 - c))
    mine.wait()
    tps(lambda tt: done_recv(mixed_copy(tt, tt)))
    tile = min(512, model)

    def project(i, _):
        at = pl.ds(pl.multiple_of(i * tile, tile), tile)
        mix_ref[:, at] = narrow(
            mm(mixed_in[...], wo_all[:, :, :, at].reshape(T * width, tile))
        )
        return 0

    lax.fori_loop(0, model // tile, project, 0)

    tps(lambda tt: done_recv(line_copy(tt, tt)))
    result = jnp.zeros((16, half), f32)
    for tt in range(T):
        result = result + line_in[tt].astype(f32)
    exp_ref[...] = narrow(jnp.concatenate([result[:8], result[8:]], axis=1))

    zs(lambda zz: done_send(tok_copy(z, zz)))

    def drain(zz, _):
        for copy in (row_copy, wo_copy):
            pl.when((zz <= z) & (z + 1 < Z))(lambda: done_send(copy(zz, 1)))
            pl.when((zz >= z) & (z >= 1))(lambda: done_send(copy(zz, -1)))
        done_send(row_sibling(zz, c))
        done_send(wo_sibling(zz, c))

        @pl.when(zz != z)
        def _():
            eps(others, lambda ee: done_send(wo_peer(zz, e, ee)))

        return 0

    lax.fori_loop(0, Z, drain, 0)
    eps(others, lambda ee: done_send(tok_peer(e, ee)))
    eps(lambda ee: e >= 0, lambda ee: done_send(tok_sibling(ee, c)))
    eps(lambda ee: e < ee, lambda ee: done_send(state_copy(e, ee)))
    eps(others, lambda ee: done_send(part_copy(e, ee)))
    tps(lambda tt: done_send(line_copy(t, tt)))
    tps(lambda tt: done_send(mixed_copy(t, tt)))


def body(
    mixer_input_rows,
    mixer_norm_gain,
    query_weight,
    key_weight,
    value_weight,
    write_strength_projection,
    decay_projection,
    head_decay_speed,
    largest_write_strength,
    extra_log_decay,
    head_norm_gain,
    mixer_output_weight,
    expert_input_rows,
    expert_norm_gain,
    routes,
    expert_route_weight,
    gate_weight,
    up_weight,
    down_weight,
):
    EP, T = lax.axis_size("ep"), lax.axis_size("tp")
    Z = T // CORES
    H = head_decay_speed.shape[0]
    hp = 4 * -(-H // 4)
    width = H * HEAD
    block, model = mixer_input_rows.shape
    toks = expert_input_rows.shape[0]
    half = model // 2
    hidden = gate_weight.shape[2]
    first = lax.axis_index("tp") * H
    assert block == BLOCK and toks == 8

    def stack(a, b):
        rest = [(0, 0)] * (a.ndim - 1)
        return jnp.concatenate(
            [jnp.pad(a, [(0, hp - H)] + rest), jnp.pad(b, [(0, hp - H)] + rest)], axis=0
        )

    w8 = stack(
        lax.dynamic_slice_in_dim(write_strength_projection.T, first, H, 0),
        lax.dynamic_slice_in_dim(decay_projection.T, first, H, 0),
    )
    prm = jnp.broadcast_to(
        stack(largest_write_strength, head_decay_speed)[:, None], (2 * hp, HEAD)
    )
    extra = jnp.pad(extra_log_decay.T, ((hp, hp - H), (0, 0)))
    lanes = lax.broadcasted_iota(jnp.int32, (toks, HEAD), 1)
    share = jnp.zeros((toks, HEAD), f32)
    for j in range(routes.shape[1]):
        share = share + jnp.where(
            lanes == routes[:, j : j + 1], expert_route_weight[:, j : j + 1], 0.0
        )

    vmem = pl.BlockSpec(memory_space=pltpu.VMEM)
    anywhere = pl.BlockSpec(memory_space=pl.ANY)
    dma = pltpu.SemaphoreType.DMA
    V = pltpu.VMEM
    return pl.pallas_call(
        functools.partial(fused_kernel, (EP, Z, H)),
        in_specs=[vmem] * 9 + [anywhere] * 7,
        out_specs=[vmem, vmem],
        out_shape=[
            jax.ShapeDtypeStruct((block, model), bf16),
            jax.ShapeDtypeStruct((toks, model), bf16),
        ],
        scratch_shapes=[
            V((model, width), bf16),
            V((model, width), bf16),
            V((model, width), bf16),
            V((model, hidden), bf16),
            V((model, hidden), bf16),
            V((hidden, model), bf16),
            V((Z, CORES, BLOCK, model), bf16),
            V((Z, CORES, width, model), bf16),
            V((EP, CORES, Z, 16, half + HEAD), bf16),
            V((EP, CORES, Z, 16, half), bf16),
            V((EP, CORES, Z, 16, half), bf16),
            V((CORES, Z, 16, half), bf16),
            V((T, 16, half), bf16),
            V((Z, CORES * BLOCK, width), f32),
            V((Z, CORES * BLOCK, width), bf16),
            V((Z, H, HEAD, 2 * HEAD), f32),
            V((Z, H, HEAD, 2 * HEAD), bf16),
            V((H, HEAD, 2 * HEAD), f32),
            V((H, HEAD, 2 * HEAD), bf16),
            V((EP, H, HEAD, 2 * HEAD), bf16),
            V((H, HEAD, HEAD), f32),
            V((T, BLOCK, width), bf16),
            V((BLOCK, T * width), bf16),
            dma((8,)),
            dma((2, Z)),
            dma((Z,)),
            dma((Z,)),
            dma((Z,)),
            dma((2, Z)),
            dma((Z,)),
            dma((Z, EP)),
            dma((Z, EP)),
            dma((Z,)),
            dma((Z,)),
            dma((Z,)),
            dma((Z,)),
            dma((EP,)),
            dma((EP,)),
            dma((EP,)),
            dma((EP,)),
            dma((EP,)),
            dma((EP,)),
            dma((EP,)),
            dma((EP,)),
            dma((T,)),
            dma((T,)),
            dma((T,)),
            dma((T,)),
        ],
        compiler_params=pltpu.CompilerParams(
            collective_id=0, has_side_effects=True, vmem_limit_bytes=60 * 1024 * 1024
        ),
    )(
        mixer_input_rows,
        mixer_norm_gain.reshape(1, model),
        w8,
        prm,
        extra,
        head_norm_gain.reshape(1, HEAD),
        expert_input_rows,
        expert_norm_gain.reshape(1, model),
        share,
        query_weight,
        key_weight,
        value_weight,
        mixer_output_weight,
        gate_weight,
        up_weight,
        down_weight,
    )


def solution(mesh):
    placed = (
        P(("ep", "tp"), None),
        P(),
        P(None, "tp"),
        P(None, "tp"),
        P(None, "tp"),
        P(),
        P(),
        P("tp"),
        P("tp"),
        P("ep", "tp"),
        P(),
        P("tp", None),
        P(("ep", "tp"), None),
        P(),
        P(("ep", "tp"), None),
        P(("ep", "tp"), None),
        P("ep", None, "tp"),
        P("ep", None, "tp"),
        P("ep", "tp", None),
    )
    return jax.shard_map(
        body,
        mesh=mesh,
        in_specs=placed,
        out_specs=(P(("ep", "tp"), None), P(("ep", "tp"), None)),
        check_vma=False,
    )
```

profile of v0, /device:TPU:5, one launch (start us, length us, event | category | flops | bytes accessed | tf_op | source)
XLA Modules:
  0.0 112.6 jit_solution(10467344353178787757)
XLA Ops:
  0.6 0.7 fusion.3
  1.4 0.8 slice_bitcast_fusion.3
  2.1 0.8 slice_bitcast_fusion.2
  2.9 0.7 select_add_fusion.share_ref
  3.6 0.6 broadcast_in_dim.28.prm_ref
  4.2 0.8 dynamic-slice_bitcast_fusion
  5.0 0.6 fusion.2.w8_ref
  5.6 1.3 %pad.22.extra_ref = f32[8,1024]{1,0:T(8,128)} pad(f32[2,1024]{1,0:T(2,128)} %bitcast.18, f32[]{:T(128)} %constant.14.clone.1), padding=4_2x0_0 | pad | bytes 40964 | tf_op jit(solution)/shard_map/jit(_pad)/pad | solution.py:651
  7.0 102.4 %shard_map.194 = (bf16[128,2048]{1,0:T(8,128)(2,1)}, bf16[8,2048]{1,0:T(8,128)(2,1)}) custom-call(bf16[128,2048]{1,0:T(8,128)(2,1)} %x_ref.1, f32[1,2048]{1,0:T(1,128)} %bitcast.16, bf16[8,2048]{1,0:T(8,128)(2,1)} %fusion.2.w8_ref, f32[8,128]{1,0:T(8,128)} %broadcast_in_dim.28.prm_ref, f32[8,1024]{1,0:T(8,128)} %pad.22.extra_ref, f32[1,128]{1,0:T(1,128)} %bitcast.19, ...), custom_call_target="tpu_custom_call" | custom-call | tf_op jit(solution)/shard_map/pallas_call | solution.py:663
  109.4 1.9 %copy.23 = bf16[128,2048]{1,0:T(8,128)(2,1)} copy(bf16[128,2048]{1,0:T(8,128)(2,1)} %get-tuple-element.10) | data formatting | bytes 1048576
  111.3 1.4 %copy.24 = bf16[8,2048]{1,0:T(8,128)(2,1)} copy(bf16[8,2048]{1,0:T(8,128)(2,1)} %get-tuple-element.11) | data formatting | bytes 65536
where the time goes:
time: 113 us
  Pallas kernels  102 us (90%)
  local copies, waits for them, and re-layouts  7.53 us (7%)
  other arithmetic  2.05 us (2%)
    pallas_call x1, Pallas kernels, body(): pl.pallas_call(functools.partial(fused_kernel, (EP, Z, H)), in_specs=[vme...  102 us
    unnamed x2, local copies, waits for them, and re-layouts  3.26 us

commit v1 on v0

--- a/solution.py
+++ b/solution.py
@@ -65,13 +65,16 @@
     sizes,
     x_ref,
     xgain_ref,
-    w8_ref,
-    prm_ref,
+    wst_ref,
+    wdt_ref,
+    largest_ref,
+    speed_ref,
     extra_ref,
     hgain_ref,
     tok_ref,
     tgain_ref,
-    share_ref,
+    routes_ref,
+    weigh_ref,
     wq_hbm,
     wk_hbm,
     wv_hbm,
@@ -81,6 +84,7 @@
     wd_hbm,
     mix_ref,
     exp_ref,
+    wsmall_ref,
     wq_ref,
     wk_ref,
     wv_ref,
@@ -91,6 +95,8 @@
     wo_all,
     tok_all,
     part_all,
+    part_sib,
+    part_sum,
     part_in,
     line_all,
     line_in,
@@ -102,6 +108,7 @@
     span_out,
     span_in,
     memory_ref,
+    total_ref,
     mixed_all,
     mixed_in,
     local_sem,
@@ -113,6 +120,8 @@
     w_r,
     wx_s,
     wx_r,
+    wh_s,
+    wh_r,
     ws_s,
     ws_r,
     t_s,
@@ -123,6 +132,8 @@
     ts_r,
     st_s,
     st_r,
+    ps_s,
+    ps_r,
     p_s,
     p_r,
     l_s,
@@ -140,7 +151,8 @@
     model = x_ref.shape[1]
     piece = model // EP
     half = model // 2
-    hp = w8_ref.shape[0] // 2
+    hp = 4 * -(-H // 4)
+    relayed = EP == 4
 
     def remote(src, dst, s, r, **where):
         return pltpu.make_async_remote_copy(
@@ -182,9 +194,20 @@
         slot = wo_slot(zz, c, frm)
         return remote(slot, slot, wx_s.at[zz, to], wx_r.at[zz, frm], ep=to)
 
-    def wo_sibling(zz, core):
-        slot = wo_all.at[zz, core]
-        return remote(slot, slot, ws_s.at[zz], ws_r.at[zz], tp=z * CORES + 1 - c)
+    def wo_half(zz, ee, i):
+        rows = width // 2
+        slot = wo_all.at[
+            zz, c, i * rows : (i + 1) * rows, pl.ds(pl.multiple_of(ee * piece, piece), piece)
+        ]
+        return remote(slot, slot, wh_s.at[zz, i], wh_r.at[zz, i], ep=e ^ (2 - i))
+
+    def wo_sibling(zz, core, ee):
+        slot = wo_slot(zz, core, ee)
+        return remote(slot, slot, ws_s.at[zz, ee], ws_r.at[zz, ee], tp=z * CORES + 1 - c)
+
+    def wo_siblings(zz, core, act):
+        for ee in range(EP):
+            act(wo_sibling(zz, core, ee))
 
     def tok_copy(frm, to):
         slot = tok_all.at[e, c, frm]
@@ -198,19 +221,22 @@
         slot = tok_all.at[ee, core]
         return remote(slot, slot, ts_s.at[ee], ts_r.at[ee], tp=z * CORES + 1 - c)
 
-    def state_copy(frm, to):
-        return remote(span_out, span_in.at[frm], st_s.at[to], st_r.at[frm], ep=to)
+    def state_copy(frm, to, i):
+        return remote(
+            span_out.at[i], span_in.at[frm, i], st_s.at[to, i], st_r.at[frm, i], ep=to
+        )
+
+    def part_sibling():
+        return remote(
+            part_all.at[1 - c], part_sib, ps_s.at[0], ps_r.at[0], tp=z * CORES + 1 - c
+        )
 
     def part_copy(frm, to):
-        return remote(part_all.at[to], part_in.at[frm], p_s.at[to], p_r.at[frm], ep=to)
+        return remote(part_sum.at[to], part_in.at[frm], p_s.at[to], p_r.at[frm], ep=to)
 
     def line_copy(frm, to):
         return remote(
-            line_all.at[to % CORES, to // CORES],
-            line_in.at[frm],
-            l_s.at[to],
-            l_r.at[frm],
-            tp=to,
+            line_all.at[to], line_in.at[frm], l_s.at[to], l_r.at[frm], tp=to * CORES + c
         )
 
     def mixed_slot(frm):
@@ -232,6 +258,7 @@
             pl.when(z != zz)(functools.partial(act, zz))
 
     others = lambda ee: e != ee
+    peers = (lambda ee: (e ^ 1 == ee) | (e ^ 2 == ee)) if relayed else others
 
     loads = [
         pltpu.make_async_copy(src, dst, local_sem.at[i])
@@ -247,8 +274,6 @@
             ]
         )
     ]
-    for load in loads:
-        load.start()
 
     barrier = pltpu.get_barrier_semaphore()
 
@@ -260,10 +285,25 @@
 
     tps(greet_tp)
     eps(others, greet_ep)
+    for load in loads[:4]:
+        load.start()
 
     rows_all[z, c] = narrow(rms_rows(x_ref[...], xgain_ref[...]))
+    wsmall_ref[...] = jnp.concatenate([wst_ref[...], wdt_ref[...]], axis=0)
     tokens = rms_rows(tok_ref[...], tgain_ref[...])
-    share = share_ref[...]
+    count = tokens.shape[0]
+    diagonal = lax.broadcasted_iota(jnp.int32, (count, count), 0) == lax.broadcasted_iota(
+        jnp.int32, (count, count), 1
+    )
+    lanes = lax.broadcasted_iota(jnp.int32, (count, HEAD), 1)
+    share = jnp.zeros((count, HEAD), f32)
+    for j in range(routes_ref.shape[0]):
+
+        def column(ref):
+            line = ref[j : j + 1, :].astype(f32)
+            return jnp.sum(jnp.where(diagonal, line, 0.0), axis=1, keepdims=True)
+
+        share = share + jnp.where(lanes.astype(f32) == column(routes_ref), column(weigh_ref), 0.0)
     share_top = narrow(share).astype(f32)
     tok_all[e, c, z] = narrow(
         jnp.concatenate(
@@ -293,18 +333,40 @@
 
     def wo_arrive(zz):
         done_recv(wo_copy(zz, 1))
-        wo_forward(zz)
-        eps(others, lambda ee: start(wo_peer(zz, e, ee)))
+        eps(peers, lambda ee: start(wo_peer(zz, e, ee)))
+        start(wo_sibling(zz, c, e))
+
+    def wo_relay(zz):
+        if relayed:
+            for i in range(2):
+                done_recv(wo_peer(zz, e ^ (1 + i), e))
+                start(wo_half(zz, e ^ (1 + i), i))
+                start(wo_sibling(zz, c, e ^ (1 + i)))
 
     def wo_collect(zz):
-        eps(others, lambda ee: done_recv(wo_peer(zz, ee, ee)))
-        start(wo_sibling(zz, c))
+        if relayed:
+            for i in range(2):
+                done_recv(wo_half(zz, e ^ 3, i))
+            start(wo_sibling(zz, c, e ^ 3))
+        else:
+
+            def pass_on(ee):
+                done_recv(wo_peer(zz, ee, ee))
+                start(wo_sibling(zz, c, ee))
+
+            eps(others, pass_on)
 
     def both_sides(s, act):
         pl.when(z - s >= 0)(lambda: act(z - s))
         pl.when(z + s < Z)(lambda: act(z + s))
 
-    for load in loads[:4]:
+    row_forward(z)
+    loads[3].wait()
+    wo_forward(z)
+    wo_siblings(z, c, start)
+    for load in loads[4:]:
+        load.start()
+    for load in loads[:3]:
         load.wait()
 
     row = lax.broadcasted_iota(jnp.int32, (BLOCK, BLOCK), 0)
@@ -319,12 +381,40 @@
         q_all = silu(mm(rows, wq_ref[...]))
         k_all = silu(mm(rows, wk_ref[...]))
         v_all = silu(mm(rows, wv_ref[...]))
-        small = mm_nt(w8_ref[...], rows)
         at_rows = pl.ds(pl.multiple_of(zz * CORES * BLOCK, CORES * BLOCK), CORES * BLOCK)
-        scale = prm_ref[:, :1]
-        strength_rows = scale / (1.0 + jnp.exp(-small))
-        softplus = jnp.maximum(small, 0.0) + jnp.log1p(jnp.exp(-jnp.abs(small)))
-        decay_rows = extra_ref[:, at_rows] - scale * softplus
+        heads = wst_ref.shape[0]
+        every = mm_nt(wsmall_ref[...], rows)
+        head = lax.broadcasted_iota(jnp.int32, (2 * heads, CORES * BLOCK), 0)
+        place = lax.broadcasted_iota(jnp.int32, (2 * hp, CORES * BLOCK), 0)
+
+        def pick(first):
+            return [
+                jnp.sum(jnp.where(head == first + t * H + h, every, 0.0), axis=0, keepdims=True)
+                for h in range(H)
+            ]
+
+        def tiled(lines, first):
+            out = jnp.zeros((2 * hp, CORES * BLOCK), f32)
+            for h, line in enumerate(lines):
+                out = jnp.where(place == first + h, line, out)
+            return out
+
+        strength_rows = tiled(
+            [
+                largest_ref[:, h : h + 1] / (1.0 + jnp.exp(-v))
+                for h, v in enumerate(pick(0))
+            ],
+            0,
+        )
+        decay_rows = tiled(
+            [
+                extra_ref[h : h + 1, at_rows]
+                - speed_ref[:, h : h + 1]
+                * (jnp.maximum(v, 0.0) + jnp.log1p(jnp.exp(-jnp.abs(v))))
+                for h, v in enumerate(pick(heads))
+            ],
+            hp,
+        )
         chains = []
         for b in range(CORES):
             at = slice(b * BLOCK, (b + 1) * BLOCK)
@@ -431,40 +521,37 @@
             weigh = (weigh[:, :8] + weigh[:, 8:]).reshape(count, 1)
             hidden = narrow(silu(mm(rows, wg_ref[...])) * mm(rows, wu_ref[...]))
             partial = (mm(hidden, wd_ref[...]) * weigh).reshape(lines * T, 8, model)
-            part_all[span] = narrow(
+            both = narrow(
                 jnp.concatenate([partial[:, :, :half], partial[:, :, half:]], axis=1)
             ).reshape(lines, CORES, Z, 16, half)
+            for core in range(CORES):
+                part_all[core, span] = both[:, core]
             return 0
 
         lax.fori_loop(0, EP // lines, chunk, 0)
 
-    mid = min(2, Z - 1)
+    mid, late = min(1, Z - 1), min(2, Z - 1)
 
     def step(s, _):
-        @pl.when(s == 0)
-        def _():
-            row_forward(z)
-
         @pl.when(s >= 1)
         def _():
             both_sides(s, row_arrive)
 
-        @pl.when(s == 1)
+        @pl.when((s >= 2) & (s <= Z - 2))
         def _():
-            wo_forward(z)
-            start(wo_sibling(z, c))
-            zs(lambda zz: done_recv(tok_copy(zz, zz)))
-            eps(others, lambda ee: start(tok_peer(e, ee)))
-
-        @pl.when(s >= 2)
-        def _():
-            both_sides(s - 1, wo_arrive)
+            both_sides(s - 1, wo_forward)
 
         @pl.when(s == mid)
         def _():
             eps(others, lambda ee: done_recv(tok_peer(ee, ee)))
             eps(lambda ee: e >= 0, lambda ee: start(tok_sibling(ee, c)))
 
+        @pl.when(s == late)
+        def _():
+            done_recv(part_sibling())
+            part_sum[...] = narrow(part_all[c].astype(f32) + part_sib[...].astype(f32))
+            eps(others, lambda ee: start(part_copy(e, ee)))
+
         def side(d, _):
             zz = jnp.where(d == 0, z - s, z + s)
 
@@ -477,7 +564,24 @@
 
         lax.fori_loop(0, 2, side, 0)
 
-        pl.when(s == max(mid, Z - 2))(experts)
+        @pl.when(s == 0)
+        def _():
+            zs(lambda zz: done_recv(tok_copy(zz, zz)))
+            eps(others, lambda ee: start(tok_peer(e, ee)))
+
+        @pl.when((s >= 1) & (s <= Z - 3))
+        def _():
+            both_sides(s, wo_arrive)
+
+        @pl.when(s == mid)
+        def _():
+            experts()
+            start(part_sibling())
+
+        @pl.when((s >= 2) & (s <= Z - 2))
+        def _():
+            both_sides(s - 1, wo_relay)
+
         return 0
 
     lax.fori_loop(0, Z, step, 0)
@@ -498,12 +602,14 @@
 
     lax.fori_loop(1, Z, compose, 0)
     for h in range(H):
-        span_out[h] = narrow(run_ref[h])
-    eps(lambda ee: e < ee, lambda ee: start(state_copy(e, ee)))
-    eps(others, lambda ee: start(part_copy(e, ee)))
-    both_sides(Z - 1, wo_arrive)
-    for s in range(1, Z - 1):
-        both_sides(s, wo_collect)
+        span_out[0, h] = narrow(run_ref[h, :, :HEAD])
+        span_out[1, h] = narrow(run_ref[h, :, HEAD:])
+    eps(lambda ee: e < ee, lambda ee: start(state_copy(e, ee, 0)))
+    eps(lambda ee: (e < ee) & (e > 0), lambda ee: start(state_copy(e, ee, 1)))
+    first_left = max(1, Z - 2)
+    if Z >= 2:
+        both_sides(first_left, wo_arrive)
+        both_sides(first_left, wo_forward)
 
     def extend(zz, _):
         for h in range(H):
@@ -514,17 +620,22 @@
         return 0
 
     lax.fori_loop(1, Z, extend, 0)
+    for s in range(1, first_left):
+        both_sides(s, wo_collect)
 
     memory_ref[...] = jnp.zeros_like(memory_ref)
 
     def enter(ee):
-        done_recv(state_copy(ee, ee))
+        done_recv(state_copy(ee, ee, 0))
+        if ee == 0:
+            memory_ref[...] = span_in[0, 0].astype(f32)
+            return
+        done_recv(state_copy(ee, ee, 1))
         for h in range(H):
             top, low = halves(memory_ref[h])
-            theirs = span_in[ee, h]
-            span_map = theirs[:, HEAD:]
+            span_map = span_in[ee, 1, h]
             memory_ref[h] = (
-                theirs[:, :HEAD].astype(f32) + mm(span_map, top) + mm(span_map, low)
+                span_in[ee, 0, h].astype(f32) + mm(span_map, top) + mm(span_map, low)
             )
 
     for ee in range(EP - 1):
@@ -546,36 +657,59 @@
     tps(lambda tt: start(mixed_copy(t, tt)))
     mine = pltpu.make_async_copy(mixed_all.at[t], mixed_slot(t), local_sem.at[7])
     mine.start()
-
-    total = part_all[e].astype(f32)
-    part_in[e] = jnp.zeros_like(part_in[e])
+    for s in range(first_left + 1, Z):
+        both_sides(s, wo_arrive)
+    if Z >= 2:
+        both_sides(first_left, wo_relay)
+
     eps(others, lambda ee: done_recv(part_copy(ee, ee)))
-    for ee in range(EP):
+    part_in[e] = part_sum[e]
+    total = part_in[0].astype(f32)
+    for ee in range(1, EP):
         total = total + part_in[ee].astype(f32)
     line_all[...] = narrow(total)
-    line_in[t] = line_all[c, z]
-    tps(lambda tt: start(line_copy(t, tt)))
-
-    both_sides(Z - 1, wo_collect)
-    zs(lambda zz: done_recv(wo_sibling(zz, 1 - c)))
-    done_recv(wo_sibling(z, 1 - c))
+    line_in[z] = line_all[z]
+    zs(lambda zz: start(line_copy(z, zz)))
+
+    def project(zz):
+        for b in range(CORES):
+            tt = zz * CORES + b
+            pl.when(tt != t)(lambda: done_recv(mixed_copy(tt, tt)))
+        wo_siblings(zz, 1 - c, done_recv)
+        heads = mixed_in[:, pl.ds(pl.multiple_of(zz * CORES * width, HEAD), CORES * width)]
+        total_ref[...] += mm(heads, wo_all[zz].reshape(CORES * width, model))
+
+    total_ref[...] = jnp.zeros_like(total_ref)
+    for s in range(first_left + 1, Z):
+        both_sides(s, wo_relay)
+    if Z >= 2:
+        both_sides(first_left, wo_collect)
     mine.wait()
-    tps(lambda tt: done_recv(mixed_copy(tt, tt)))
-    tile = min(512, model)
-
-    def project(i, _):
-        at = pl.ds(pl.multiple_of(i * tile, tile), tile)
-        mix_ref[:, at] = narrow(
-            mm(mixed_in[...], wo_all[:, :, :, at].reshape(T * width, tile))
-        )
+
+    def near(s, _):
+        def side(d, _):
+            zz = jnp.where(d == 0, z - s, z + s)
+
+            @pl.when((zz >= 0) & (zz < Z) & ((s > 0) | (d == 0)))
+            def _():
+                @pl.when((s > first_left))
+                def _():
+                    wo_collect(zz)
+
+                project(zz)
+
+            return 0
+
+        lax.fori_loop(0, 2, side, 0)
         return 0
 
-    lax.fori_loop(0, model // tile, project, 0)
-
-    tps(lambda tt: done_recv(line_copy(tt, tt)))
-    result = jnp.zeros((16, half), f32)
-    for tt in range(T):
-        result = result + line_in[tt].astype(f32)
+    lax.fori_loop(0, Z, near, 0)
+    mix_ref[...] = narrow(total_ref[...])
+
+    zs(lambda zz: done_recv(line_copy(zz, zz)))
+    result = line_in[0].astype(f32)
+    for zz in range(1, Z):
+        result = result + line_in[zz].astype(f32)
     exp_ref[...] = narrow(jnp.concatenate([result[:8], result[8:]], axis=1))
 
     zs(lambda zz: done_send(tok_copy(z, zz)))
@@ -585,20 +719,25 @@
             pl.when((zz <= z) & (z + 1 < Z))(lambda: done_send(copy(zz, 1)))
             pl.when((zz >= z) & (z >= 1))(lambda: done_send(copy(zz, -1)))
         done_send(row_sibling(zz, c))
-        done_send(wo_sibling(zz, c))
+        wo_siblings(zz, c, done_send)
 
         @pl.when(zz != z)
         def _():
-            eps(others, lambda ee: done_send(wo_peer(zz, e, ee)))
+            eps(peers, lambda ee: done_send(wo_peer(zz, e, ee)))
+            if relayed:
+                for i in range(2):
+                    done_send(wo_half(zz, e ^ (1 + i), i))
 
         return 0
 
     lax.fori_loop(0, Z, drain, 0)
     eps(others, lambda ee: done_send(tok_peer(e, ee)))
     eps(lambda ee: e >= 0, lambda ee: done_send(tok_sibling(ee, c)))
-    eps(lambda ee: e < ee, lambda ee: done_send(state_copy(e, ee)))
+    eps(lambda ee: e < ee, lambda ee: done_send(state_copy(e, ee, 0)))
+    eps(lambda ee: (e < ee) & (e > 0), lambda ee: done_send(state_copy(e, ee, 1)))
     eps(others, lambda ee: done_send(part_copy(e, ee)))
-    tps(lambda tt: done_send(line_copy(t, tt)))
+    done_send(part_sibling())
+    zs(lambda zz: done_send(line_copy(z, zz)))
     tps(lambda tt: done_send(mixed_copy(t, tt)))
 
 
@@ -626,49 +765,28 @@
     EP, T = lax.axis_size("ep"), lax.axis_size("tp")
     Z = T // CORES
     H = head_decay_speed.shape[0]
-    hp = 4 * -(-H // 4)
     width = H * HEAD
     block, model = mixer_input_rows.shape
     toks = expert_input_rows.shape[0]
     half = model // 2
     hidden = gate_weight.shape[2]
-    first = lax.axis_index("tp") * H
     assert block == BLOCK and toks == 8
-
-    def stack(a, b):
-        rest = [(0, 0)] * (a.ndim - 1)
-        return jnp.concatenate(
-            [jnp.pad(a, [(0, hp - H)] + rest), jnp.pad(b, [(0, hp - H)] + rest)], axis=0
-        )
-
-    w8 = stack(
-        lax.dynamic_slice_in_dim(write_strength_projection.T, first, H, 0),
-        lax.dynamic_slice_in_dim(decay_projection.T, first, H, 0),
-    )
-    prm = jnp.broadcast_to(
-        stack(largest_write_strength, head_decay_speed)[:, None], (2 * hp, HEAD)
-    )
-    extra = jnp.pad(extra_log_decay.T, ((hp, hp - H), (0, 0)))
-    lanes = lax.broadcasted_iota(jnp.int32, (toks, HEAD), 1)
-    share = jnp.zeros((toks, HEAD), f32)
-    for j in range(routes.shape[1]):
-        share = share + jnp.where(
-            lanes == routes[:, j : j + 1], expert_route_weight[:, j : j + 1], 0.0
-        )
 
     vmem = pl.BlockSpec(memory_space=pltpu.VMEM)
     anywhere = pl.BlockSpec(memory_space=pl.ANY)
     dma = pltpu.SemaphoreType.DMA
     V = pltpu.VMEM
-    return pl.pallas_call(
+    outs = [
+        jax.ShapeDtypeStruct((block, model), bf16),
+        jax.ShapeDtypeStruct((toks, model), bf16),
+    ]
+    results = pl.pallas_call(
         functools.partial(fused_kernel, (EP, Z, H)),
-        in_specs=[vmem] * 9 + [anywhere] * 7,
+        in_specs=[vmem] * 12 + [anywhere] * 7,
         out_specs=[vmem, vmem],
-        out_shape=[
-            jax.ShapeDtypeStruct((block, model), bf16),
-            jax.ShapeDtypeStruct((toks, model), bf16),
-        ],
+        out_shape=outs,
         scratch_shapes=[
+            V((2 * write_strength_projection.shape[1], model), bf16),
             V((model, width), bf16),
             V((model, width), bf16),
             V((model, width), bf16),
@@ -678,59 +796,48 @@
             V((Z, CORES, BLOCK, model), bf16),
             V((Z, CORES, width, model), bf16),
             V((EP, CORES, Z, 16, half + HEAD), bf16),
-            V((EP, CORES, Z, 16, half), bf16),
-            V((EP, CORES, Z, 16, half), bf16),
-            V((CORES, Z, 16, half), bf16),
-            V((T, 16, half), bf16),
+            V((CORES, EP, Z, 16, half), bf16),
+            V((EP, Z, 16, half), bf16),
+            V((EP, Z, 16, half), bf16),
+            V((EP, Z, 16, half), bf16),
+            V((Z, 16, half), bf16),
+            V((Z, 16, half), bf16),
             V((Z, CORES * BLOCK, width), f32),
             V((Z, CORES * BLOCK, width), bf16),
             V((Z, H, HEAD, 2 * HEAD), f32),
             V((Z, H, HEAD, 2 * HEAD), bf16),
             V((H, HEAD, 2 * HEAD), f32),
-            V((H, HEAD, 2 * HEAD), bf16),
-            V((EP, H, HEAD, 2 * HEAD), bf16),
+            V((2, H, HEAD, HEAD), bf16),
+            V((EP, 2, H, HEAD, HEAD), bf16),
             V((H, HEAD, HEAD), f32),
+            V((BLOCK, model), f32),
             V((T, BLOCK, width), bf16),
             V((BLOCK, T * width), bf16),
             dma((8,)),
-            dma((2, Z)),
-            dma((Z,)),
-            dma((Z,)),
-            dma((Z,)),
-            dma((2, Z)),
-            dma((Z,)),
-            dma((Z, EP)),
-            dma((Z, EP)),
-            dma((Z,)),
-            dma((Z,)),
-            dma((Z,)),
-            dma((Z,)),
-            dma((EP,)),
-            dma((EP,)),
-            dma((EP,)),
-            dma((EP,)),
-            dma((EP,)),
-            dma((EP,)),
-            dma((EP,)),
-            dma((EP,)),
-            dma((T,)),
-            dma((T,)),
-            dma((T,)),
-            dma((T,)),
+            *[dma((2, Z)), dma((Z,)), dma((Z,)), dma((Z,))],
+            *[dma((2, Z)), dma((Z,)), dma((Z, EP)), dma((Z, EP))],
+            *[dma((Z, 2)), dma((Z, 2)), dma((Z, EP)), dma((Z, EP))],
+            *[dma((Z,)), dma((Z,)), dma((EP,)), dma((EP,)), dma((EP,)), dma((EP,))],
+            *[dma((EP, 2)), dma((EP, 2))],
+            *[dma((1,)), dma((1,)), dma((EP,)), dma((EP,)), dma((Z,)), dma((Z,))],
+            *[dma((T,)), dma((T,))],
         ],
         compiler_params=pltpu.CompilerParams(
-            collective_id=0, has_side_effects=True, vmem_limit_bytes=60 * 1024 * 1024
+            collective_id=0, has_side_effects=True, vmem_limit_bytes=63 * 1024 * 1024
         ),
     )(
         mixer_input_rows,
         mixer_norm_gain.reshape(1, model),
-        w8,
-        prm,
-        extra,
+        write_strength_projection.T,
+        decay_projection.T,
+        largest_write_strength.reshape(1, H),
+        head_decay_speed.reshape(1, H),
+        extra_log_decay.T,
         head_norm_gain.reshape(1, HEAD),
         expert_input_rows,
         expert_norm_gain.reshape(1, model),
-        share,
+        routes.T,
+        expert_route_weight.T,
         query_weight,
         key_weight,
         value_weight,
@@ -739,6 +846,14 @@
         up_weight,
         down_weight,
     )
+    return pl.pallas_call(
+        hand_over, in_specs=[vmem, vmem], out_specs=[vmem, vmem], out_shape=outs
+    )(*results)
+
+
+def hand_over(mix_in, exp_in, mix_out, exp_out):
+    mix_out[...] = mix_in[...]
+    exp_out[...] = exp_in[...]
 
 
 def solution(mesh):

time: 113 us -> 87.6 us (0.78)
  Pallas kernels: 102 us -> 86.2 us
  local copies, waits for them, and re-layouts: 7.53 us -> 0 us
  other arithmetic: 2.05 us -> 0 us
    pallas_call x1, Pallas kernels: 102 us -> 84.3 us  [body(): pl.pallas_call(functools.partial(fused_kernel, (EP, Z, H)), in_specs=[vme...]
    unnamed x2 -> x0, local copies, waits for them, and re-layouts: 3.26 us -> none
    pallas_call x0 -> x1, Pallas kernels: none -> 1.87 us  [body(): pl.pallas_call(hand_over, in_specs=[vmem, vmem], out_specs=[vmem, vmem],...]
    broadcast_in_dim x2 -> x0, local copies, waits for them, and re-layouts: 1.4 us -> none  [the longest x1 0.76 us: body(): jnp.where(lanes == routes[:, j:j + 1], expert_route_weight[:, j:j + 1], 0.0)]
    concatenate x2 -> x0, other arithmetic: 1.39 us -> none  [stack(): jnp.concatenate([jnp.pad(a, [(0, hp - H)] + rest), jnp.pad(b, [(0, hp - H...]
    pad x1 -> x0, local copies, waits for them, and re-layouts: 1.32 us -> none  [body(): extra = jnp.pad(extra_log_decay.T, ((hp, hp - H), (0, 0)))]
where the time goes in v1:
time: 87.6 us; the launch traced here: 86.8 us
  Pallas kernels  86.2 us (98%)
    pallas_call x1, Pallas kernels, body(): pl.pallas_call(functools.partial(fused_kernel, (EP, Z, H)), in_specs=[vme...  84.3 us
    pallas_call x1, Pallas kernels, body(): pl.pallas_call(hand_over, in_specs=[vmem, vmem], out_specs=[vmem, vmem],...  1.87 us

profile of v1, /device:TPU:5, one launch (start us, length us, event | category | flops | bytes accessed | tf_op | source)
XLA Modules:
  0.0 86.8 jit_solution(226730380539445067)
XLA Ops:
  0.6 84.3 %shard_map.194 = (bf16[128,2048]{1,0:T(8,128)(2,1)}, bf16[8,2048]{1,0:T(8,128)(2,1)}) custom-call(bf16[128,2048]{1,0:T(8,128)(2,1)} %x_ref.1, f32[1,2048]{1,0:T(1,128)} %bitcast.12, bf16[16,2048]{1,0:T(8,128)(2,1)} %bitcast.10, bf16[16,2048]{1,0:T(8,128)(2,1)} %bitcast.11, f32[1,2]{1,0:T(1,128)} %bitcast.17, f32[1,2]{1,0:T(1,128)} %bitcast.18, ...), custom_call_target="tpu_custom_call" | custom-call | tf_op jit(solution)/shard_map/pallas_call | solution.py:783
  85.0 1.9 %shard_map.195 = (bf16[128,2048]{1,0:T(8,128)(2,1)}, bf16[8,2048]{1,0:T(8,128)(2,1)}) custom-call(bf16[128,2048]{1,0:T(8,128)(2,1)} %get-tuple-element.4.mix_in, bf16[8,2048]{1,0:T(8,128)(2,1)} %get-tuple-element.5.exp_in), custom_call_target="tpu_custom_call" | custom-call | tf_op jit(solution)/shard_map/pallas_call | solution.py:849

commit v2 on v1

--- a/solution.py
+++ b/solution.py
@@ -61,8 +61,28 @@
     return wide * lax.rsqrt(jnp.mean(wide * wide, axis=-1, keepdims=True) + norm_eps) * gain
 
 
+SMALL = 12
+
+
+def loading_kernel(sizes, *refs):
+    raw, rest = refs[:SMALL], refs[SMALL:]
+    placed, tiles, sem, others = rest[:9], rest[9 : 9 + SMALL], rest[9 + SMALL], rest[10 + SMALL :]
+
+    def load():
+        copies = [
+            pltpu.make_async_copy(src, dst, sem.at[i])
+            for i, (src, dst) in enumerate(zip(raw, tiles))
+        ]
+        for copy in copies:
+            copy.start()
+        return copies
+
+    fused_kernel(sizes, load, *tiles, *placed, *others)
+
+
 def fused_kernel(
     sizes,
+    load_small,
     x_ref,
     xgain_ref,
     wst_ref,
@@ -182,32 +202,33 @@
         slot = rows_all.at[zz, core]
         return remote(slot, slot, rs_s.at[zz], rs_r.at[zz], tp=z * CORES + 1 - c)
 
-    def wo_slot(zz, core, ee):
-        return wo_all.at[zz, core, :, pl.ds(pl.multiple_of(ee * piece, piece), piece)]
-
-    def wo_copy(zz, step):
-        slot = wo_slot(zz, c, e)
+    def wo_slot(zz, core, ee, i):
+        rows = width // 2
+        return wo_all.at[
+            zz, core, i * rows : (i + 1) * rows, pl.ds(pl.multiple_of(ee * piece, piece), piece)
+        ]
+
+    def wo_copy(zz, step, i):
+        slot = wo_slot(zz, c, e, i)
         d = 0 if step > 0 else 1
-        return remote(slot, slot, w_s.at[d, zz], w_r.at[zz], tp=t + step * CORES)
-
-    def wo_peer(zz, frm, to):
-        slot = wo_slot(zz, c, frm)
-        return remote(slot, slot, wx_s.at[zz, to], wx_r.at[zz, frm], ep=to)
+        return remote(slot, slot, w_s.at[d, zz, i], w_r.at[zz, i], tp=t + step * CORES)
+
+    def wo_peer(zz, frm, to, i):
+        slot = wo_slot(zz, c, frm, i)
+        return remote(slot, slot, wx_s.at[zz, to, i], wx_r.at[zz, frm, i], ep=to)
 
     def wo_half(zz, ee, i):
-        rows = width // 2
-        slot = wo_all.at[
-            zz, c, i * rows : (i + 1) * rows, pl.ds(pl.multiple_of(ee * piece, piece), piece)
-        ]
+        slot = wo_slot(zz, c, ee, i)
         return remote(slot, slot, wh_s.at[zz, i], wh_r.at[zz, i], ep=e ^ (2 - i))
 
-    def wo_sibling(zz, core, ee):
-        slot = wo_slot(zz, core, ee)
-        return remote(slot, slot, ws_s.at[zz, ee], ws_r.at[zz, ee], tp=z * CORES + 1 - c)
+    def wo_sibling(zz, core, ee, i):
+        slot = wo_slot(zz, core, ee, i)
+        return remote(slot, slot, ws_s.at[zz, ee, i], ws_r.at[zz, ee, i], tp=z * CORES + 1 - c)
 
     def wo_siblings(zz, core, act):
         for ee in range(EP):
-            act(wo_sibling(zz, core, ee))
+            for i in range(2):
+                act(wo_sibling(zz, core, ee, i))
 
     def tok_copy(frm, to):
         slot = tok_all.at[e, c, frm]
@@ -285,8 +306,11 @@
 
     tps(greet_tp)
     eps(others, greet_ep)
+    small = load_small()
     for load in loads[:4]:
         load.start()
+    for load in small:
+        load.wait()
 
     rows_all[z, c] = narrow(rms_rows(x_ref[...], xgain_ref[...]))
     wsmall_ref[...] = jnp.concatenate([wst_ref[...], wdt_ref[...]], axis=0)
@@ -327,32 +351,52 @@
         done_recv(row_copy(zz, 1))
         row_forward(zz)
 
-    def wo_forward(zz):
-        pl.when((zz <= z) & (z + 1 < Z))(lambda: start(wo_copy(zz, 1)))
-        pl.when((zz >= z) & (z >= 1))(lambda: start(wo_copy(zz, -1)))
-
-    def wo_arrive(zz):
-        done_recv(wo_copy(zz, 1))
-        eps(peers, lambda ee: start(wo_peer(zz, e, ee)))
-        start(wo_sibling(zz, c, e))
+    end = (z == 0) | (z == Z - 1)
+    early_left, early_right = end | (z < Z // 2), end | (z >= Z // 2)
+
+    def wo_out(early):
+        for i in range(2):
+            pl.when((z + 1 < Z) & (early_right == early))(lambda: start(wo_copy(z, 1, i)))
+            pl.when((z >= 1) & (early_left == early))(lambda: start(wo_copy(z, -1, i)))
+
+    def sides(early, s, act):
+        pl.when((z - s >= 0) & (early_left == early))(lambda: act(z - s))
+        pl.when((z + s < Z) & (early_right == early))(lambda: act(z + s))
+
+
+    def wo_arrive(zz, which=(0, 1)):
+        for i in which:
+            done_recv(wo_copy(zz, 1, i))
+            pl.when((zz < z) & (z + 1 < Z))(lambda: start(wo_copy(zz, 1, i)))
+            pl.when((zz > z) & (z >= 1))(lambda: start(wo_copy(zz, -1, i)))
+            if relayed:
+                start(wo_peer(zz, e, e ^ (1 + i), i))
+                start(wo_peer(zz, e, e ^ (2 - i), i))
+            else:
+                eps(others, lambda ee: start(wo_peer(zz, e, ee, i)))
+            start(wo_sibling(zz, c, e, i))
 
     def wo_relay(zz):
         if relayed:
             for i in range(2):
-                done_recv(wo_peer(zz, e ^ (1 + i), e))
+                done_recv(wo_peer(zz, e ^ (1 + i), e, i))
                 start(wo_half(zz, e ^ (1 + i), i))
-                start(wo_sibling(zz, c, e ^ (1 + i)))
+                start(wo_sibling(zz, c, e ^ (1 + i), i))
 
     def wo_collect(zz):
         if relayed:
             for i in range(2):
+                done_recv(wo_peer(zz, e ^ (1 + i), e, 1 - i))
+                start(wo_sibling(zz, c, e ^ (1 + i), 1 - i))
+            for i in range(2):
                 done_recv(wo_half(zz, e ^ 3, i))
-            start(wo_sibling(zz, c, e ^ 3))
+                start(wo_sibling(zz, c, e ^ 3, i))
         else:
 
             def pass_on(ee):
-                done_recv(wo_peer(zz, ee, ee))
-                start(wo_sibling(zz, c, ee))
+                for i in range(2):
+                    done_recv(wo_peer(zz, ee, ee, i))
+                    start(wo_sibling(zz, c, ee, i))
 
             eps(others, pass_on)
 
@@ -362,7 +406,7 @@
 
     row_forward(z)
     loads[3].wait()
-    wo_forward(z)
+    wo_out(True)
     wo_siblings(z, c, start)
     for load in loads[4:]:
         load.start()
@@ -372,7 +416,10 @@
     row = lax.broadcasted_iota(jnp.int32, (BLOCK, BLOCK), 0)
     col = lax.broadcasted_iota(jnp.int32, (BLOCK, BLOCK), 1)
 
-    def process(zz):
+    first_left = max(1, Z - 2)
+    midway = Z >= 3
+
+    def process(zz, s):
         causal = row >= col
         strict = row > col
         eye = (row == col).astype(f32)
@@ -452,6 +499,12 @@
         pair_mask = strict & (row // 2 == col // 2)
         for m in chains:
             m["inv"] = eye - jnp.where(pair_mask, m["low"], 0.0)
+        if midway:
+
+            @pl.when(s == Z - 1)
+            def _():
+                both_sides(first_left, lambda other: wo_arrive(other, (0,)))
+
         size = 2
         while size < BLOCK:
             mask = (row // (2 * size) == col // (2 * size)) & (row // size > col // size)
@@ -537,12 +590,9 @@
         def _():
             both_sides(s, row_arrive)
 
-        @pl.when((s >= 2) & (s <= Z - 2))
-        def _():
-            both_sides(s - 1, wo_forward)
-
         @pl.when(s == mid)
         def _():
+            wo_out(False)
             eps(others, lambda ee: done_recv(tok_peer(ee, ee)))
             eps(lambda ee: e >= 0, lambda ee: start(tok_sibling(ee, c)))
 
@@ -558,7 +608,7 @@
             @pl.when((zz >= 0) & (zz < Z) & ((s > 0) | (d == 0)))
             def _():
                 done_recv(row_sibling(zz, 1 - c))
-                process(zz)
+                process(zz, s)
 
             return 0
 
@@ -571,7 +621,7 @@
 
         @pl.when((s >= 1) & (s <= Z - 3))
         def _():
-            both_sides(s, wo_arrive)
+            sides(True, s, wo_arrive)
 
         @pl.when(s == mid)
         def _():
@@ -580,7 +630,8 @@
 
         @pl.when((s >= 2) & (s <= Z - 2))
         def _():
-            both_sides(s - 1, wo_relay)
+            sides(False, s - 1, wo_arrive)
+            sides(True, s - 1, wo_relay)
 
         return 0
 
@@ -604,12 +655,14 @@
     for h in range(H):
         span_out[0, h] = narrow(run_ref[h, :, :HEAD])
         span_out[1, h] = narrow(run_ref[h, :, HEAD:])
-    eps(lambda ee: e < ee, lambda ee: start(state_copy(e, ee, 0)))
-    eps(lambda ee: (e < ee) & (e > 0), lambda ee: start(state_copy(e, ee, 1)))
-    first_left = max(1, Z - 2)
-    if Z >= 2:
+    for ee in reversed(range(EP)):
+        pl.when(e < ee)(lambda: start(state_copy(e, ee, 0)))
+        pl.when((e < ee) & (e > 0))(lambda: start(state_copy(e, ee, 1)))
+    if midway:
+        pl.when(end)(lambda: both_sides(first_left, lambda zz: wo_arrive(zz, (1,))))
+        pl.when(~end)(lambda: both_sides(first_left, wo_arrive))
+    elif Z >= 2:
         both_sides(first_left, wo_arrive)
-        both_sides(first_left, wo_forward)
 
     def extend(zz, _):
         for h in range(H):
@@ -620,8 +673,6 @@
         return 0
 
     lax.fori_loop(1, Z, extend, 0)
-    for s in range(1, first_left):
-        both_sides(s, wo_collect)
 
     memory_ref[...] = jnp.zeros_like(memory_ref)
 
@@ -641,7 +692,19 @@
     for ee in range(EP - 1):
         pl.when(ee < e)(functools.partial(enter, ee))
 
-    def finish(zz, _):
+    def put_off(tt):
+        return ((tt // CORES) % (Z - 1) == 0) & (z % (Z - 1) != 0) if Z > 2 else t < 0
+
+    def send_heads(zz):
+        for b in range(CORES):
+            tt = zz * CORES + b
+            pl.when((tt != t) & ~put_off(tt))(lambda: start(mixed_copy(t, tt)))
+
+    def turn(i):
+        return lax.rem(z + Z // 2 + i, Z)
+
+    def finish(i, _):
+        zz = turn(i)
         for h in range(H):
             of = slice(h * HEAD, (h + 1) * HEAD)
             top, low = halves(memory_ref[h])
@@ -651,14 +714,17 @@
             done = narrow(heads * scale * hgain_ref[...])
             for b in range(CORES):
                 mixed_all[zz * CORES + b, :, of] = done[b * BLOCK : (b + 1) * BLOCK]
+        pl.when(i > 0)(lambda: send_heads(turn(i - 1)))
         return 0
 
     lax.fori_loop(0, Z, finish, 0)
-    tps(lambda tt: start(mixed_copy(t, tt)))
+    send_heads(turn(Z - 1))
     mine = pltpu.make_async_copy(mixed_all.at[t], mixed_slot(t), local_sem.at[7])
     mine.start()
     for s in range(first_left + 1, Z):
         both_sides(s, wo_arrive)
+    for s in range(1, first_left):
+        sides(False, s, wo_relay)
     if Z >= 2:
         both_sides(first_left, wo_relay)
 
@@ -680,10 +746,11 @@
         total_ref[...] += mm(heads, wo_all[zz].reshape(CORES * width, model))
 
     total_ref[...] = jnp.zeros_like(total_ref)
+    tps(lambda tt: pl.when(put_off(tt))(lambda: start(mixed_copy(t, tt))))
     for s in range(first_left + 1, Z):
         both_sides(s, wo_relay)
-    if Z >= 2:
-        both_sides(first_left, wo_collect)
+    for s in range(1, first_left + 1):
+        both_sides(s, wo_collect)
     mine.wait()
 
     def near(s, _):
@@ -715,15 +782,16 @@
     zs(lambda zz: done_send(tok_copy(z, zz)))
 
     def drain(zz, _):
-        for copy in (row_copy, wo_copy):
-            pl.when((zz <= z) & (z + 1 < Z))(lambda: done_send(copy(zz, 1)))
-            pl.when((zz >= z) & (z >= 1))(lambda: done_send(copy(zz, -1)))
+        for right in (lambda step: row_copy(zz, step), lambda step: wo_copy(zz, step, 0), lambda step: wo_copy(zz, step, 1)):
+            pl.when((zz <= z) & (z + 1 < Z))(lambda: done_send(right(1)))
+            pl.when((zz >= z) & (z >= 1))(lambda: done_send(right(-1)))
         done_send(row_sibling(zz, c))
         wo_siblings(zz, c, done_send)
 
         @pl.when(zz != z)
         def _():
-            eps(peers, lambda ee: done_send(wo_peer(zz, e, ee)))
+            for i in range(2):
+                eps(peers, lambda ee: done_send(wo_peer(zz, e, ee, i)))
             if relayed:
                 for i in range(2):
                     done_send(wo_half(zz, e ^ (1 + i), i))
@@ -780,52 +848,7 @@
         jax.ShapeDtypeStruct((block, model), bf16),
         jax.ShapeDtypeStruct((toks, model), bf16),
     ]
-    results = pl.pallas_call(
-        functools.partial(fused_kernel, (EP, Z, H)),
-        in_specs=[vmem] * 12 + [anywhere] * 7,
-        out_specs=[vmem, vmem],
-        out_shape=outs,
-        scratch_shapes=[
-            V((2 * write_strength_projection.shape[1], model), bf16),
-            V((model, width), bf16),
-            V((model, width), bf16),
-            V((model, width), bf16),
-            V((model, hidden), bf16),
-            V((model, hidden), bf16),
-            V((hidden, model), bf16),
-            V((Z, CORES, BLOCK, model), bf16),
-            V((Z, CORES, width, model), bf16),
-            V((EP, CORES, Z, 16, half + HEAD), bf16),
-            V((CORES, EP, Z, 16, half), bf16),
-            V((EP, Z, 16, half), bf16),
-            V((EP, Z, 16, half), bf16),
-            V((EP, Z, 16, half), bf16),
-            V((Z, 16, half), bf16),
-            V((Z, 16, half), bf16),
-            V((Z, CORES * BLOCK, width), f32),
-            V((Z, CORES * BLOCK, width), bf16),
-            V((Z, H, HEAD, 2 * HEAD), f32),
-            V((Z, H, HEAD, 2 * HEAD), bf16),
-            V((H, HEAD, 2 * HEAD), f32),
-            V((2, H, HEAD, HEAD), bf16),
-            V((EP, 2, H, HEAD, HEAD), bf16),
-            V((H, HEAD, HEAD), f32),
-            V((BLOCK, model), f32),
-            V((T, BLOCK, width), bf16),
-            V((BLOCK, T * width), bf16),
-            dma((8,)),
-            *[dma((2, Z)), dma((Z,)), dma((Z,)), dma((Z,))],
-            *[dma((2, Z)), dma((Z,)), dma((Z, EP)), dma((Z, EP))],
-            *[dma((Z, 2)), dma((Z, 2)), dma((Z, EP)), dma((Z, EP))],
-            *[dma((Z,)), dma((Z,)), dma((EP,)), dma((EP,)), dma((EP,)), dma((EP,))],
-            *[dma((EP, 2)), dma((EP, 2))],
-            *[dma((1,)), dma((1,)), dma((EP,)), dma((EP,)), dma((Z,)), dma((Z,))],
-            *[dma((T,)), dma((T,))],
-        ],
-        compiler_params=pltpu.CompilerParams(
-            collective_id=0, has_side_effects=True, vmem_limit_bytes=63 * 1024 * 1024
-        ),
-    )(
+    small = [
         mixer_input_rows,
         mixer_norm_gain.reshape(1, model),
         write_strength_projection.T,
@@ -838,6 +861,57 @@
         expert_norm_gain.reshape(1, model),
         routes.T,
         expert_route_weight.T,
+    ]
+    scratch = [
+        *[V(v.shape, v.dtype) for v in small],
+        dma((SMALL,)),
+        V((2 * write_strength_projection.shape[1], model), bf16),
+        V((model, width), bf16),
+        V((model, width), bf16),
+        V((model, width), bf16),
+        V((model, hidden), bf16),
+        V((model, hidden), bf16),
+        V((hidden, model), bf16),
+        V((Z, CORES, BLOCK, model), bf16),
+        V((Z, CORES, width, model), bf16),
+        V((EP, CORES, Z, 16, half + HEAD), bf16),
+        V((CORES, EP, Z, 16, half), bf16),
+        V((EP, Z, 16, half), bf16),
+        V((EP, Z, 16, half), bf16),
+        V((EP, Z, 16, half), bf16),
+        V((Z, 16, half), bf16),
+        V((Z, 16, half), bf16),
+        V((Z, CORES * BLOCK, width), f32),
+        V((Z, CORES * BLOCK, width), bf16),
+        V((Z, H, HEAD, 2 * HEAD), f32),
+        V((Z, H, HEAD, 2 * HEAD), bf16),
+        V((H, HEAD, 2 * HEAD), f32),
+        V((2, H, HEAD, HEAD), bf16),
+        V((EP, 2, H, HEAD, HEAD), bf16),
+        V((H, HEAD, HEAD), f32),
+        V((BLOCK, model), f32),
+        V((T, BLOCK, width), bf16),
+        V((BLOCK, T * width), bf16),
+        dma((8,)),
+        *[dma((2, Z)), dma((Z,)), dma((Z,)), dma((Z,))],
+        *[dma((2, Z, 2)), dma((Z, 2)), dma((Z, EP, 2)), dma((Z, EP, 2))],
+        *[dma((Z, 2)), dma((Z, 2)), dma((Z, EP, 2)), dma((Z, EP, 2))],
+        *[dma((Z,)), dma((Z,)), dma((EP,)), dma((EP,)), dma((EP,)), dma((EP,))],
+        *[dma((EP, 2)), dma((EP, 2))],
+        *[dma((1,)), dma((1,)), dma((EP,)), dma((EP,)), dma((Z,)), dma((Z,))],
+        *[dma((T,)), dma((T,))],
+    ]
+    results = pl.pallas_call(
+        functools.partial(loading_kernel, (EP, Z, H)),
+        in_specs=[anywhere] * (SMALL + 7),
+        out_specs=[vmem, vmem],
+        out_shape=outs,
+        scratch_shapes=scratch,
+        compiler_params=pltpu.CompilerParams(
+            collective_id=0, has_side_effects=True, vmem_limit_bytes=63 << 20
+        ),
+    )(
+        *small,
         query_weight,
         key_weight,
         value_weight,
@@ -847,13 +921,23 @@
         down_weight,
     )
     return pl.pallas_call(
-        hand_over, in_specs=[vmem, vmem], out_specs=[vmem, vmem], out_shape=outs
+        hand_over,
+        in_specs=[vmem, vmem],
+        out_specs=[anywhere, anywhere],
+        out_shape=outs,
+        scratch_shapes=[dma((2,))],
     )(*results)
 
 
-def hand_over(mix_in, exp_in, mix_out, exp_out):
-    mix_out[...] = mix_in[...]
-    exp_out[...] = exp_in[...]
+def hand_over(mix_in, exp_in, mix_out, exp_out, sem):
+    copies = [
+        pltpu.make_async_copy(mix_in, mix_out, sem.at[0]),
+        pltpu.make_async_copy(exp_in, exp_out, sem.at[1]),
+    ]
+    for copy in copies:
+        copy.start()
+    for copy in copies:
+        copy.wait()
 
 
 def solution(mesh):

time: 87.6 us -> 85.3 us (0.974)
  Pallas kernels: 86.2 us -> 84.1 us
    pallas_call x2, Pallas kernels: 86.2 us -> 84.1 us  [the longest x1 82.3 us: body(): pl.pallas_call(functools.partial(loading_kernel, (EP, Z, H)), in_specs=[a...]
where the time goes in v2:
time: 85.3 us; the launch traced here: 84.8 us
  Pallas kernels  84.1 us (99%)
    pallas_call x1, Pallas kernels, body(): pl.pallas_call(functools.partial(loading_kernel, (EP, Z, H)), in_specs=[a...  82.3 us
    pallas_call x1, Pallas kernels, body(): pl.pallas_call(hand_over, in_specs=[vmem, vmem], out_specs=[anywhere, any...  1.86 us

profile of v2, /device:TPU:5, one launch (start us, length us, event | category | flops | bytes accessed | tf_op | source)
XLA Modules:
  0.0 84.8 jit_solution(13008991887573514486)
XLA Ops:
  0.6 82.3 %shard_map.194 = (bf16[128,2048]{1,0:T(8,128)(2,1)}, bf16[8,2048]{1,0:T(8,128)(2,1)}) custom-call(bf16[128,2048]{1,0:T(8,128)(2,1)} %refs_0_.1, f32[1,2048]{1,0:T(1,128)} %bitcast.12, bf16[16,2048]{1,0:T(8,128)(2,1)} %bitcast.10, bf16[16,2048]{1,0:T(8,128)(2,1)} %bitcast.11, f32[1,2]{1,0:T(1,128)} %bitcast.17, f32[1,2]{1,0:T(1,128)} %bitcast.18, ...), custom_call_target="tpu_custom_call" | custom-call | tf_op jit(solution)/shard_map/pallas_call | solution.py:904
  82.9 1.9 %shard_map.195 = (bf16[128,2048]{1,0:T(8,128)(2,1)}, bf16[8,2048]{1,0:T(8,128)(2,1)}) custom-call(bf16[128,2048]{1,0:T(8,128)(2,1)} %get-tuple-element.4.mix_in, bf16[8,2048]{1,0:T(8,128)(2,1)} %get-tuple-element.5.exp_in), custom_call_target="tpu_custom_call" | custom-call | tf_op jit(solution)/shard_map/pallas_call | solution.py:923

commit v3 on v2

--- a/solution.py
+++ b/solution.py
@@ -674,6 +674,9 @@
 
     lax.fori_loop(1, Z, extend, 0)
 
+    for s in range(first_left + 1, Z):
+        both_sides(s, wo_arrive)
+
     memory_ref[...] = jnp.zeros_like(memory_ref)
 
     def enter(ee):
@@ -721,8 +724,6 @@
     send_heads(turn(Z - 1))
     mine = pltpu.make_async_copy(mixed_all.at[t], mixed_slot(t), local_sem.at[7])
     mine.start()
-    for s in range(first_left + 1, Z):
-        both_sides(s, wo_arrive)
     for s in range(1, first_left):
         sides(False, s, wo_relay)
     if Z >= 2:

time: 85.3 us -> 84.3 us (0.988)
  Pallas kernels: 84.1 us -> 83.1 us
    pallas_call x1, Pallas kernels: 82.3 us -> 81.3 us  [body(): pl.pallas_call(functools.partial(loading_kernel, (EP, Z, H)), in_specs=[a...]
where the time goes in v3:
time: 84.3 us; the launch traced here: 83.8 us
  Pallas kernels  83.1 us (99%)
    pallas_call x1, Pallas kernels, body(): pl.pallas_call(functools.partial(loading_kernel, (EP, Z, H)), in_specs=[a...  81.3 us
    pallas_call x1, Pallas kernels, body(): pl.pallas_call(hand_over, in_specs=[vmem, vmem], out_specs=[anywhere, any...  1.86 us

profile of v3, /device:TPU:5, one launch (start us, length us, event | category | flops | bytes accessed | tf_op | source)
XLA Modules:
  0.0 83.8 jit_solution(12597429362645044574)
XLA Ops:
  0.6 81.3 %shard_map.194 = (bf16[128,2048]{1,0:T(8,128)(2,1)}, bf16[8,2048]{1,0:T(8,128)(2,1)}) custom-call(bf16[128,2048]{1,0:T(8,128)(2,1)} %refs_0_.1, f32[1,2048]{1,0:T(1,128)} %bitcast.12, bf16[16,2048]{1,0:T(8,128)(2,1)} %bitcast.10, bf16[16,2048]{1,0:T(8,128)(2,1)} %bitcast.11, f32[1,2]{1,0:T(1,128)} %bitcast.17, f32[1,2]{1,0:T(1,128)} %bitcast.18, ...), custom_call_target="tpu_custom_call" | custom-call | tf_op jit(solution)/shard_map/pallas_call | solution.py:905
  81.9 1.9 %shard_map.195 = (bf16[128,2048]{1,0:T(8,128)(2,1)}, bf16[8,2048]{1,0:T(8,128)(2,1)}) custom-call(bf16[128,2048]{1,0:T(8,128)(2,1)} %get-tuple-element.4.mix_in, bf16[8,2048]{1,0:T(8,128)(2,1)} %get-tuple-element.5.exp_in), custom_call_target="tpu_custom_call" | custom-call | tf_op jit(solution)/shard_map/pallas_call | solution.py:924
